TPU v7x, 32 devices: a whole 2x2x4 slice. The times are simulated.
32 devices in a mesh: sp: 16 (over z, y, x), tp: 2 (over core).
Axes of the slice: x: 2, y: 2, z: 4, core: 2. Of those that a mesh axis runs over, the one named last changes fastest.
Arguments:
- queries: bfloat16 [8192, 2048], P('sp', 'tp'), may hold values from -6 to 6
- keys: bfloat16 [8192, 1024], P('sp', 'tp'), may hold values from -6 to 6
- values: bfloat16 [8192, 1024], P('sp', 'tp'), may hold values from -6 to 6
- documents: int32 [8192], P('sp'), may hold values from 0 to 3, never falling along the last dimension, each value on 1 to 4096 neighbouring positions
- query_gain: float32 [128], replicated, may hold values from 1.8 to 6
- key_gain: float32 [128], replicated, may hold values from 1.8 to 6
- residual: bfloat16 [8192, 4096], P('sp', 'tp'), may hold values from -6 to 6
- out_weight: bfloat16 [2048, 4096], P('tp'), may hold values from -0.125 to 0.125
- norm_gain: float32 [4096], replicated, may hold values from 0.1 to 1.9
- up_weight: bfloat16 [4096, 16384], P('sp', 'tp'), may hold values from -0.09375 to 0.09375
- down_weight: bfloat16 [16384, 4096], P('tp', 'sp'), may hold values from -0.046875 to 0.046875
Outputs:
- mixed: bfloat16 [8192, 4096], P('sp', 'tp')
Inputs may be any that keep to these rules, and one draw needn't show every extreme that they name: `documents`: document numbers never fall along the sequence; a document has at most 4096 positions.
All inputs are finite; a program needn't handle non-finite values.
Results may differ from a plain program's by a relative error of at most 0.017.
The roundings to bfloat16 on the way count: a program that leaves them out, or rounds other values in their place, can miss the bound.
Values may be sent and summed in bfloat16 or wider, within the bound.
A program may use at most 256 MiB of HBM per device.

v0:
```python
import functools

import jax
import jax.numpy as jnp
from jax import lax
from jax.experimental import pallas as pl
from jax.experimental.layout import Layout, with_layout_constraint
from jax.experimental.pallas import tpu as pltpu
from jax.sharding import PartitionSpec as P


HQ = 16
KV = 8
HD = 128
GRID_W = 64


norm_eps = 1e-06
rope_base = 10000.0
masked_score = -1e30
log2e = 1.4426950408889634


def head_norm(heads_in, gain):
    values32 = heads_in.astype(jnp.float32)
    scaled = values32 * lax.rsqrt(jnp.mean(values32 * values32, axis=-1, keepdims=True) + norm_eps)
    return scaled * gain


def rotate_half(heads_in, position):
    quarter = heads_in.shape[-1] // 2
    inverse_freq = rope_base ** (-jnp.arange(quarter, dtype=jnp.float32) / quarter)
    angles = position[:, None] * inverse_freq[None, :]
    cosine_part = jnp.cos(angles)[:, None, :]
    sine_part = jnp.sin(angles)[:, None, :]
    leading = heads_in[..., :quarter]
    trailing = heads_in[..., quarter:]
    return jnp.concatenate(
        [
            leading * cosine_part - trailing * sine_part,
            leading * sine_part + trailing * cosine_part,
        ],
        axis=-1,
    )


def grid_rotary(heads_in, positions):
    half_width = heads_in.shape[-1] // 2
    grid_row = (positions // GRID_W).astype(jnp.float32)
    grid_col = (positions % GRID_W).astype(jnp.float32)
    return jnp.concatenate(
        [
            rotate_half(heads_in[..., :half_width], grid_row),
            rotate_half(heads_in[..., half_width:], grid_col),
        ],
        axis=-1,
    )


def row_major(array):
    return with_layout_constraint(array, Layout(major_to_minor=(0, 1)))


def from_behind(array, shift, size):
    return lax.ppermute(array, "tp", [(i, (i + shift) % size) for i in range(size)])


def gather_body(
    queries,
    keys,
    values,
    documents,
    query_gain,
    key_gain,
    residual,
    out_weight,
    norm_gain,
    up_weight,
    down_weight,
):
    tok_rows = queries.shape[0]
    key_heads = keys.shape[1] // HD
    group_size = HQ // KV
    width_local = residual.shape[1]
    tp_index = lax.axis_index("tp")
    up_whole = lax.all_gather(up_weight, "sp", axis=0, tiled=True)
    tp_size = lax.axis_size("tp")
    residual_whole = jnp.zeros((tok_rows, width_local * tp_size), jnp.bfloat16)
    residual_whole = lax.dynamic_update_slice_in_dim(
        residual_whole, residual, tp_index * width_local, 1
    )
    for shift in range(1, tp_size):
        owner = (tp_index - shift) % tp_size
        residual_whole = lax.dynamic_update_slice_in_dim(
            residual_whole, from_behind(residual, shift, tp_size), owner * width_local, 1
        )
    positions = lax.axis_index("sp") * tok_rows + jnp.arange(tok_rows, dtype=jnp.int32)
    queries_rot = grid_rotary(
        head_norm(queries.reshape(tok_rows, key_heads * group_size, HD), query_gain), positions
    )
    queries_rot = queries_rot.astype(jnp.bfloat16).reshape(tok_rows, key_heads, group_size, HD)
    keys_rot = grid_rotary(
        head_norm(keys.reshape(tok_rows, key_heads, HD), key_gain), positions
    ).astype(jnp.bfloat16)
    value_heads = values.reshape(tok_rows, key_heads, HD)
    own_docs = documents.astype(jnp.bfloat16)
    score_scale = HD ** (-0.5)
    key_value = jnp.concatenate(
        [keys_rot.reshape(tok_rows, key_heads * HD), value_heads.reshape(tok_rows, key_heads * HD)],
        axis=1,
    )
    key_value = lax.all_gather(key_value, "sp", axis=0, tiled=True)
    doc_piece = lax.all_gather(own_docs, "sp", axis=0, tiled=True)
    same_doc = own_docs[:, None] == doc_piece[None, :]
    head_queries = queries_rot.reshape(tok_rows, key_heads * group_size, HD).swapaxes(0, 1)

    def attend(query_head):
        head, query = query_head
        key_at = head // group_size * HD
        key_piece = lax.dynamic_slice_in_dim(key_value, key_at, HD, 1)
        value_piece = lax.dynamic_slice_in_dim(key_value, key_at + key_heads * HD, HD, 1)
        scores = jnp.einsum("qd,sd->qs", query, key_piece, preferred_element_type=jnp.float32)
        scores = jnp.where(same_doc, scores * score_scale, masked_score)
        row_max = jnp.max(scores, axis=-1, keepdims=True)
        probs = jnp.where(same_doc, jnp.exp(scores - row_max), 0.0)
        row_sum = jnp.sum(probs, axis=-1)
        update = jnp.dot(
            probs.astype(jnp.bfloat16), value_piece, preferred_element_type=jnp.float32
        )
        return (update / row_sum[:, None]).astype(jnp.bfloat16)

    attended = lax.map(attend, (jnp.arange(key_heads * group_size), head_queries))
    down_late, attended = lax.optimization_barrier((row_major(down_weight.T), attended))
    down_whole = lax.all_gather(down_late, "sp", axis=0, tiled=True)
    attended = attended.swapaxes(0, 1)
    attended = attended.reshape(tok_rows, key_heads * group_size * HD)
    partial_out = jnp.dot(attended, out_weight, preferred_element_type=jnp.float32)
    partial_out = partial_out.astype(jnp.bfloat16)
    branch = partial_out.astype(jnp.float32)
    for shift in range(1, tp_size):
        branch = branch + from_behind(partial_out, shift, tp_size).astype(jnp.float32)
    stream_whole = residual_whole.astype(jnp.float32) + branch
    normed = stream_whole * lax.rsqrt(
        jnp.mean(stream_whole * stream_whole, axis=-1, keepdims=True) + norm_eps
    )
    normed = (normed * norm_gain).astype(jnp.bfloat16)
    stream = lax.dynamic_slice_in_dim(stream_whole, tp_index * width_local, width_local, 1)
    hidden = jnp.dot(normed, up_whole, preferred_element_type=jnp.float32)
    positive = jnp.maximum(hidden, 0.0)
    squared = (positive * positive).astype(jnp.bfloat16)
    product = lax.dot_general(
        squared, down_whole, (((1,), (1,)), ((), ())), preferred_element_type=jnp.float32
    )
    product = product.astype(jnp.bfloat16)
    feed = lax.dynamic_slice_in_dim(product, tp_index * width_local, width_local, 1)
    feed = feed.astype(jnp.float32)
    for shift in range(1, tp_size):
        target = (tp_index + shift) % tp_size
        piece = lax.dynamic_slice_in_dim(product, target * width_local, width_local, 1)
        feed = feed + from_behind(piece, shift, tp_size).astype(jnp.float32)
    return (stream + feed).astype(jnp.bfloat16)


def prepare_kernel(heads, group, q_ref, k_ref, v_ref, cos_ref, sin_ref, qg_ref, kg_ref, o_ref):
    cosine = cos_ref[...]
    sine = sin_ref[...]
    lane = lax.broadcasted_iota(jnp.int32, cosine.shape, 1)
    first = (lane % (HD // 2)) < HD // 4

    def turned(u, gain):
        u = u.astype(jnp.float32)
        u = u * lax.rsqrt(jnp.mean(u * u, axis=-1, keepdims=True) + norm_eps) * gain
        ahead = pltpu.roll(u, HD - HD // 4, 1)
        behind = pltpu.roll(u, HD // 4, 1)
        return (u * cosine + jnp.where(first, ahead, behind) * sine).astype(jnp.bfloat16)

    q_gain = qg_ref[...]
    k_gain = kg_ref[...]
    for h in range(heads):
        for g in range(group):
            at = (h * group + g) * HD
            o_ref[h, :, g * HD : (g + 1) * HD] = turned(q_ref[:, at : at + HD], q_gain)
        at = h * HD
        o_ref[h, :, group * HD : (group + 1) * HD] = turned(k_ref[:, at : at + HD], k_gain)
        o_ref[h, :, (group + 1) * HD :] = v_ref[:, at : at + HD]


def prepare(queries, keys, values, positions, query_gain, key_gain):
    rows = queries.shape[0]
    heads = keys.shape[1] // HD
    group = HQ // KV
    lane = jnp.arange(HD, dtype=jnp.int32)
    quarter = HD // 4
    freq = rope_base ** (-(lane % quarter).astype(jnp.float32) / quarter)
    grid_row = (positions // GRID_W).astype(jnp.float32)
    grid_col = (positions % GRID_W).astype(jnp.float32)
    where_at = jnp.where(lane[None, :] < HD // 2, grid_row[:, None], grid_col[:, None])
    angles = where_at * freq[None, :]
    cosine = jnp.cos(angles)
    sine = jnp.where((lane % (HD // 2)) < quarter, -1.0, 1.0)[None, :] * jnp.sin(angles)
    block = min(rows, 128)
    width = (group + 2) * HD
    row_block = lambda cols: pl.BlockSpec((block, cols), lambda i: (i, 0))
    fixed = pl.BlockSpec((1, HD), lambda i: (0, 0))
    return pl.pallas_call(
        functools.partial(prepare_kernel, heads, group),
        grid=(rows // block,),
        out_shape=jax.ShapeDtypeStruct((heads, rows, width), jnp.bfloat16),
        in_specs=[
            row_block(heads * group * HD),
            row_block(heads * HD),
            row_block(heads * HD),
            row_block(HD),
            row_block(HD),
            fixed,
            fixed,
        ],
        out_specs=pl.BlockSpec((heads, block, width), lambda i: (0, i, 0)),
        cost_estimate=pl.CostEstimate(flops=rows * 20000, bytes_accessed=rows * 8192, transcendentals=0),
        name="prepare",
    )(queries, keys, values, cosine, sine, query_gain.reshape(1, HD), key_gain.reshape(1, HD))


def attend_kernel(group, key_block, slots, span_ref, q_ref, kv_ref, qdoc_ref, kdoc_ref, o_ref):
    tile = pl.program_id(0)
    lo = span_ref[0, tile]
    hi = span_ref[1, tile]
    plane = span_ref[4, tile]
    rows = q_ref.shape[0]
    per_slot = kv_ref.shape[0] // slots
    query = jnp.concatenate([q_ref[:, g * HD : (g + 1) * HD] for g in range(group)], axis=0)
    q_doc = jnp.concatenate([qdoc_ref[...]] * group, axis=0)
    factor = HD ** (-0.5) * log2e

    def step(block, carry):
        top, total, out = carry
        slot = lax.rem(plane + slots - block // per_slot, slots)
        at = slot * per_slot + lax.rem(block, per_slot)
        key = kv_ref[at, :key_block, :HD]
        value = kv_ref[at, :key_block, HD:]
        scores = lax.dot_general(
            query, key, (((1,), (1,)), ((), ())), preferred_element_type=jnp.float32
        )
        k_doc = kdoc_ref[block]
        scores = jnp.where(q_doc == k_doc, scores, masked_score)
        new_top = jnp.maximum(top, jnp.max(scores, axis=-1, keepdims=True))
        probs = jnp.exp2((scores - new_top) * factor)
        fade = jnp.exp2((top - new_top) * factor)
        total = total * fade + jnp.sum(probs, axis=-1, keepdims=True)
        out = out * fade + jnp.dot(
            probs.astype(jnp.bfloat16), value, preferred_element_type=jnp.float32
        )
        return new_top, total, out

    start = (
        jnp.full((group * rows, 1), masked_score, jnp.float32),
        jnp.zeros((group * rows, 1), jnp.float32),
        jnp.zeros((group * rows, HD), jnp.float32),
    )
    _, total, out = lax.fori_loop(lo, hi, step, start)
    out = (out / total).astype(jnp.bfloat16)
    for g in range(group):
        o_ref[:, g * HD : (g + 1) * HD] = out[g * rows : (g + 1) * rows]


doc_pad = 16


def attention(packed, key_value, docs, plane, group, slots):
    rows = packed.shape[0]
    tile = min(256, rows)
    key_block = key_value.shape[1] - doc_pad
    own = lax.dynamic_slice_in_dim(docs, plane * rows, rows)
    q_low = own[::tile]
    q_high = own[tile - 1 :: tile]
    k_low = docs[::key_block]
    k_high = docs[key_block - 1 :: key_block]
    lo = jnp.sum(k_high[None, :] < q_low[:, None], axis=1).astype(jnp.int32)
    hi = jnp.sum(k_low[None, :] <= q_high[:, None], axis=1).astype(jnp.int32)
    span = jnp.stack([lo, hi, q_low, q_high, jnp.full_like(lo, plane)])
    blocks = docs.shape[0] // key_block
    grid_spec = pltpu.PrefetchScalarGridSpec(
        num_scalar_prefetch=1,
        grid=(rows // tile,),
        in_specs=[
            pl.BlockSpec((tile, group * HD), lambda i, s: (i, 0)),
            pl.BlockSpec(key_value.shape, lambda i, s: (0, 0, 0)),
            pl.BlockSpec((tile, 1), lambda i, s: (i, 0)),
            pl.BlockSpec((blocks, 1, key_block), lambda i, s: (0, 0, 0)),
        ],
        out_specs=pl.BlockSpec((tile, group * HD), lambda i, s: (i, 0)),
    )
    work = group * rows * docs.shape[0] // 2
    return pl.pallas_call(
        functools.partial(attend_kernel, group, key_block, slots),
        grid_spec=grid_spec,
        out_shape=jax.ShapeDtypeStruct((rows, group * HD), jnp.bfloat16),
        compiler_params=pltpu.CompilerParams(vmem_limit_bytes=48 * 1024 * 1024),
        cost_estimate=pl.CostEstimate(
            flops=work * 4 * HD, bytes_accessed=key_value.size * 2, transcendentals=work
        ),
        name="attention",
    )(span, packed, key_value, own.reshape(rows, 1), docs.reshape(blocks, 1, key_block))


MESH = pl.DeviceIdType.MESH


def feed_kernel(
    outer, inner, tok, width, units,
    normed_ref, up_own, up_odd, down_own, late_u2, late_d2, late_d3, late_d1,
    own_ref, ends_ref, mids_ref, last_ref, tok_a, tok_b, given_s, given_r, send_e, send_x, send_l, land_u, land_d,
    up_v, down_v, tok_v, sq_v, stage_v, recv_v, add_v, sum_v,
    way_s, way_r, pair_s, pair_r, give_s, give_r, e_s, e_r, x_s, x_r, l_s, l_r, w_s, w_r, loc, big,
):
    me = lax.axis_index("sp")
    core = lax.axis_index("tp")
    z = me // inner
    i = me % inner
    mid = ((z + 1) // 2) % 2
    near = (z + 1 - 2 * (z % 2)) * inner + i
    across = (outer - 1 - z) * inner + i
    half = tok // 2

    barrier = pltpu.get_barrier_semaphore()
    beside = [{"sp": z * inner + i + bit - 2 * bit * ((i // bit) % 2)} for bit in (1, 2)]
    for peer in ({"sp": near}, {"sp": across}, {"tp": 1 - core}, *beside):
        pl.semaphore_signal(barrier, inc=1, device_id=peer, device_id_type=MESH)
    pl.semaphore_wait(barrier, 5)

    def remote(src, dst, send, recv, peer):
        return pltpu.make_async_remote_copy(
            src_ref=src, dst_ref=dst, send_sem=send, recv_sem=recv, device_id=peer, device_id_type=MESH
        )

    def local(src, dst, sem):
        copy = pltpu.make_async_copy(src, dst, sem)
        copy.start()
        copy.wait()

    to_near, to_across, to_core = {"sp": near}, {"sp": across}, {"tp": 1 - core}
    own_near = remote(normed_ref, tok_a.at[1], way_s.at[0], way_r.at[1], to_near)
    own_across = remote(normed_ref, tok_a.at[3], way_s.at[1], way_r.at[3], to_across)
    near_across = remote(tok_a.at[1], tok_a.at[2], way_s.at[2], way_r.at[2], to_across)
    across_near = remote(tok_a.at[3], tok_a.at[2], way_s.at[3], way_r.at[2], to_near)
    far_near = remote(tok_a.at[2], tok_a.at[3], way_s.at[4], way_r.at[3], to_near)

    def token_pair(q):
        src = normed_ref if isinstance(q, int) and q == 0 else tok_a.at[q]
        return remote(src, tok_b.at[q], pair_s.at[q], pair_r.at[q], to_core)

    def arrived(q):
        remote(tok_a.at[q], tok_a.at[q], way_s.at[0], way_r.at[q], to_near).wait_recv()
        token_pair(q).start()

    own_near.start()
    token_pair(0).start()
    depth = late_u2.shape[0]
    plane_of = (z, z + 1 - 2 * (z % 2), (z + 2) % 4, 3 - z)
    peers = {bit: {"sp": z * inner + i + bit - 2 * bit * ((i // bit) % 2)} for bit in (1, 2)}
    items = [
        (late_u2, land_u, 2, (1, 2)),
        (late_d2, land_d.at[0], 2, (2, 1)),
        (late_d3, land_d.at[1], 3, (1, 2)),
        (late_d1, land_d.at[2], 1, (2, 1)),
    ]

    def leg(n, j):
        src, land, _, (first, second) = items[n]
        from_ref = src if j < 3 else land.at[first - 1]
        return remote(
            from_ref, land.at[j - 1], w_s.at[n, j - 1], w_r.at[n, j - 1], peers[second if j == 3 else j]
        )

    def send_item(n):
        first, second = items[n][3]
        leg(n, first).start()
        leg(n, second).start()

    def forward_item(n):
        leg(n, items[n][3][0]).wait_recv()
        leg(n, 3).start()

    def into(weights, plane, j, src, sem):
        at = pl.ds(pl.multiple_of((plane * inner + j) * depth, depth), depth)
        dst = up_v.at[at] if weights == 0 else down_v.at[:, at]
        return pltpu.make_async_copy(src, dst, sem)

    loads = [], []
    for j in range(inner):
        loads[0].append(into(0, plane_of[0], j, up_own.at[j], big.at[0, 0, j]))
        for n, k in enumerate((1, 3)):
            src = up_odd.at[j, n * depth : (n + 1) * depth]
            loads[0].append(into(0, plane_of[k], j, src, big.at[0, k, j]))
        loads[1].append(into(1, plane_of[0], j, down_own.at[j], big.at[1, 0, j]))
    flipped = (i, i + 1 - 2 * (i % 2), (i + 2) % 4, 3 - i)

    def item_loads(n):
        src, land, k, _ = items[n]
        weights = 0 if n == 0 else 1
        copies = [into(weights, plane_of[k], i, src, big.at[weights, k, 0])]
        for j in range(1, inner):
            copies.append(
                into(weights, plane_of[k], flipped[j], land.at[j - 1], big.at[weights, k, j])
            )
        return copies

    def land_item(n):
        leg(n, items[n][3][1]).wait_recv()
        leg(n, 3).wait_recv()
        copies = item_loads(n)
        for copy in copies:
            copy.start()
        return copies

    send_item(0)
    send_item(1)
    for copy in loads[0] + loads[1]:
        copy.start()

    @pl.when(mid == 1)
    def _():
        own_across.start()

    def given_pair(q):
        return remote(given_s.at[q], given_r.at[q], give_s.at[q], give_r.at[q], to_core)

    block = 512

    def hide(q, first=False):
        src = normed_ref if first else tok_a.at[q]
        own_in = pltpu.make_async_copy(src, tok_v.at[core], loc.at[0])
        own_in.start()
        token_pair(q).wait_recv()
        other_in = pltpu.make_async_copy(tok_b.at[q], tok_v.at[1 - core], loc.at[1])
        other_in.start()
        own_in.wait()
        other_in.wait()

        @pl.loop(0, units // block)
        def _(n):
            cols = pl.ds(pl.multiple_of(n * block, block), block)
            hidden = jnp.dot(tok_v[0], up_v[:width, cols], preferred_element_type=jnp.float32)
            hidden += jnp.dot(tok_v[1], up_v[width:, cols], preferred_element_type=jnp.float32)
            hidden = jnp.maximum(hidden, 0.0)
            sq_v[q, :, cols] = (hidden * hidden).astype(jnp.bfloat16)

    def keep_rows(q, start, size):
        return pl.ds(pl.multiple_of(q * tok + start, size), size)

    def multiply(q):
        def product(side, put):
            @pl.loop(0, width // block)
            def _(n):
                from_at = pl.multiple_of(side * width + n * block, block)
                part = jnp.dot(
                    sq_v[q], down_v[:, pl.ds(from_at, block)], preferred_element_type=jnp.float32
                )
                put(pl.ds(pl.multiple_of(n * block, block), block), part.astype(jnp.bfloat16))

        def put_stage(cols, part):
            stage_v[:, cols] = part

        def put_keep(cols, part):
            up_v[keep_rows(q, 0, tok), cols] = part

        product(1 - core, put_stage)
        local(stage_v, given_s.at[q], loc.at[2])
        given_pair(q).start()
        product(core, put_keep)

    chunk = 128

    def total(q, start, extra):
        rows = pl.ds(start, chunk)
        value = up_v[keep_rows(q, start, chunk)].astype(jnp.float32)
        value = value + recv_v[rows].astype(jnp.float32)
        if extra:
            value = value + add_v[rows].astype(jnp.float32)
        return value

    def pass_on(q, extra, wait, out, copies):
        given_pair(q).wait_recv()
        one = pltpu.make_async_copy(given_r.at[q], recv_v, loc.at[3])
        one.start()
        one.wait()
        for h in range(2):
            rows = pl.ds(h * half, half)
            if extra is not None:
                wait(h)
                local(extra.at[rows], add_v.at[rows], loc.at[4])

            @pl.loop(0, half // chunk)
            def _(n):
                start = pl.multiple_of(h * half + n * chunk, chunk)
                sum_v[pl.ds(start, chunk)] = total(q, start, extra is not None).astype(jnp.bfloat16)

            local(sum_v.at[rows], out.at[rows], loc.at[5])
            copies(h).start()

    def halves(src, dst, send, recv, peer):
        def copy(h):
            rows = pl.ds(h * half, half)
            return remote(src.at[rows], dst.at[rows], send.at[h], recv.at[h], peer)

        return copy

    to_mid = [
        halves(send_e.at[n], ends_ref.at[n], e_s.at[n], e_r.at[n], to_near) for n in range(3)
    ]
    to_other = [
        halves(send_x.at[n], mids_ref.at[n], x_s.at[n], x_r.at[n], to_across) for n in range(2)
    ]
    to_end = halves(send_l, last_ref, l_s, l_r, to_near)

    forward_item(0)
    forward_item(1)
    send_item(2)
    send_item(3)
    arrived(1)

    @pl.when(mid == 1)
    def _():
        near_across.start()
        arrived(3)
        across_near.start()

    for copy in land_item(0) + loads[0]:
        copy.wait()
    hide(0, True)
    hide(1)
    forward_item(2)
    forward_item(3)
    landed = land_item(1)

    @pl.when(mid == 0)
    def _():
        arrived(2)

    hide(2 + mid)

    @pl.when(mid == 1)
    def _():
        arrived(2)
        far_near.start()

    @pl.when(mid == 0)
    def _():
        arrived(3)

    hide(3 - mid)
    landed = landed + land_item(2) + land_item(3)
    for copy in landed + loads[1]:
        copy.wait()
    multiply(1)

    @pl.when(mid == 0)
    def _():
        pass_on(1, None, None, send_e.at[0], to_mid[0])

    multiply(2 + mid)

    @pl.when(mid == 0)
    def _():
        pass_on(2, None, None, send_e.at[1], to_mid[1])

    multiply(3 - mid)

    @pl.when(mid == 0)
    def _():
        pass_on(3, None, None, send_e.at[2], to_mid[2])

    multiply(0)

    @pl.when(mid == 1)
    def _():
        pass_on(3, ends_ref.at[1], lambda h: to_mid[1](h).wait_recv(), send_x.at[0], to_other[0])
        pass_on(2, ends_ref.at[2], lambda h: to_mid[2](h).wait_recv(), send_x.at[1], to_other[1])
        pass_on(1, mids_ref.at[1], lambda h: to_other[1](h).wait_recv(), send_l, to_end)

    given_pair(0).wait_recv()
    local(given_r.at[0], recv_v, loc.at[3])

    @pl.loop(0, tok // chunk)
    def _(n):
        start = pl.multiple_of(n * chunk, chunk)
        sum_v[pl.ds(start, chunk)] = total(0, start, False).astype(jnp.bfloat16)

    local(sum_v, own_ref, loc.at[5])

    @pl.when(mid == 0)
    def _():
        for h in range(2):
            to_end(h).wait_recv()
            for n in range(3):
                to_mid[n](h).wait_send()

    @pl.when(mid == 1)
    def _():
        own_across.wait_send()
        near_across.wait_send()
        across_near.wait_send()
        far_near.wait_send()
        for h in range(2):
            to_mid[0](h).wait_recv()
            to_other[0](h).wait_recv()
            for n in range(2):
                to_other[n](h).wait_send()
            to_end(h).wait_send()

    own_near.wait_send()
    for n in range(len(items)):
        for j in range(1, inner):
            leg(n, j).wait_send()
    for q in range(outer):
        token_pair(q).wait_send()
        given_pair(q).wait_send()


def feed_forward(normed, up_own, up_odd, down_own, late, inner, outer):
    tok, width = normed.shape
    depth, units = late[0].shape
    block = lambda *lead: jax.ShapeDtypeStruct(lead + (tok, width), jnp.bfloat16)
    any_space = pl.BlockSpec(memory_space=pl.ANY)
    outs = [block(), block(3), block(2), block()]
    outs += [block(outer), block(outer), block(outer), block(outer), block(3), block(2), block()]
    outs += [
        jax.ShapeDtypeStruct((inner - 1, depth, units), jnp.bfloat16),
        jax.ShapeDtypeStruct((3, inner - 1, units, depth), jnp.bfloat16),
    ]
    dma = pltpu.SemaphoreType.DMA
    vmem = lambda *shape: pltpu.VMEM(shape, jnp.bfloat16)
    flops = 8 * outer * tok * width * units
    return pl.pallas_call(
        functools.partial(feed_kernel, outer, inner, tok, width, units),
        out_shape=outs,
        in_specs=[any_space] * (4 + len(late)),
        out_specs=[any_space] * len(outs),
        scratch_shapes=[
            vmem(2 * width, units),
            vmem(units, 2 * width),
            vmem(2, tok, width),
            vmem(outer, tok, units),
            vmem(tok, width),
            vmem(tok, width),
            vmem(tok, width),
            vmem(tok, width),
            dma((5,)), dma((outer,)), dma((outer,)), dma((outer,)), dma((outer,)), dma((outer,)),
            dma((3, 2)), dma((3, 2)), dma((2, 2)), dma((2, 2)), dma((2,)), dma((2,)),
            dma((4, inner - 1)), dma((4, inner - 1)), dma((6,)), dma((2, outer, inner)),
        ],
        compiler_params=pltpu.CompilerParams(
            collective_id=0, has_side_effects=True, vmem_limit_bytes=63 * 1024 * 1024
        ),
        cost_estimate=pl.CostEstimate(flops=flops, bytes_accessed=0, transcendentals=0),
        name="feed_forward",
    )(normed, up_own, up_odd, down_own, *late)[:4]


def split_body(
    inner,
    outer,
    queries,
    keys,
    values,
    documents,
    query_gain,
    key_gain,
    residual,
    out_weight,
    norm_gain,
    up_weight,
    down_weight,
):
    tok = queries.shape[0]
    group = HQ // KV
    width = residual.shape[1]
    units = up_weight.shape[1] // outer
    size = inner * outer
    me = lax.axis_index("sp")
    core = lax.axis_index("tp")
    z = me // inner
    i = me % inner

    def flip(array, bits):
        return lax.ppermute(array, "sp", [(s, s ^ bits) for s in range(size)])

    def partner(array):
        return lax.ppermute(array, "tp", [(0, 1), (1, 0)])

    def line(array, step):
        pairs = [
            (s, s + step * inner) for s in range(size) if 0 <= s // inner + step < outer
        ]
        return lax.ppermute(array, "sp", pairs)

    def gather_line(array):
        right, left = [array], [array]
        for _ in range(1, outer):
            right.append(line(right[-1], 1))
            left.append(line(left[-1], -1))
        return [array] + [
            jnp.where(z >= r, right[r], left[outer - r]) for r in range(1, outer)
        ]

    def after(array, *others):
        return lax.optimization_barrier((array,) + others)[0]

    planes = [[p * inner + j for j in range(inner)] for p in range(outer)]

    def spread(block):
        return lax.all_gather(block, "sp", axis=0, axis_index_groups=planes, tiled=False)

    positions = me * tok + jnp.arange(tok, dtype=jnp.int32)
    packed = prepare(queries, keys, values, positions, query_gain, key_gain)
    cols = 2 * HD
    doc_rows = tok // cols
    notes = jnp.zeros((doc_pad, (group + 2) * HD), jnp.bfloat16)
    notes = notes.at[:doc_rows, group * HD :].set(
        documents.astype(jnp.bfloat16).reshape(doc_rows, cols)
    )
    notes = jnp.broadcast_to(notes[None], (inner,) + notes.shape)
    packed = jnp.concatenate([packed, notes], axis=1)

    def moved(weight, k, axis, *gates):
        block = lax.dynamic_slice_in_dim(weight, (z ^ k) * units, units, axis)
        if gates:
            block = after(block, *gates)
        return flip(block, k * inner)

    early_1 = moved(up_weight, 1, 1)
    early_3 = moved(up_weight, 3, 1)

    mine = jnp.zeros((inner,) + packed.shape[1:], jnp.bfloat16)
    for m in range(inner):
        piece = lax.dynamic_index_in_dim(packed, i ^ m, 0, keepdims=False)
        if m:
            piece = flip(piece, m)
        mine = lax.dynamic_update_index_in_dim(mine, piece, i ^ m, 0)
    key_slots = gather_line(mine[:, :, group * HD :].reshape(-1, cols))
    key_value = jnp.stack(key_slots)

    up_own = spread(after(lax.dynamic_slice_in_dim(up_weight, z * units, units, 1), mine))
    up_odd = spread(jnp.concatenate([after(early_1, key_value), early_3], axis=0))
    down_own = spread(
        after(lax.dynamic_slice_in_dim(down_weight, z * units, units, 0), key_value)
    )
    late_u2 = moved(up_weight, 2, 1, key_value)
    late_d2 = moved(down_weight, 2, 0, key_value)
    late_d3 = moved(down_weight, 3, 0, key_value)
    late_d1 = moved(down_weight, 1, 0, key_value)

    docs = key_value.reshape(outer, inner, tok + doc_pad, cols)[:, :, tok : tok + doc_rows]
    docs = docs.reshape(outer, inner * tok).astype(jnp.int32)
    docs = docs[(z - jnp.arange(outer)) % outer].reshape(-1)
    attended = attention(
        mine[:, :tok].reshape(inner * tok, -1),
        key_value.reshape(outer * inner, tok + doc_pad, cols),
        docs, z, group, outer,
    )
    attended = attended.reshape(inner, tok, group * HD)
    pieces, rows = [], []
    for m in range(inner):
        piece = lax.dynamic_index_in_dim(attended, i ^ m, 0, keepdims=False)
        pieces.append(flip(piece, m) if m else piece)
        rows.append(lax.dynamic_slice_in_dim(out_weight, (i ^ m) * group * HD, group * HD, 0))
    rows = after(jnp.concatenate(rows, axis=0), packed)
    heads = jnp.concatenate(pieces, axis=1)
    partial_out = jnp.dot(heads, rows, preferred_element_type=jnp.float32)
    partial_out = partial_out.astype(jnp.bfloat16)
    kept = lax.dynamic_slice_in_dim(partial_out, core * width, width, 1)
    given = lax.dynamic_slice_in_dim(partial_out, (1 - core) * width, width, 1)
    branch = kept.astype(jnp.float32) + partner(given).astype(jnp.float32)
    stream = residual.astype(jnp.float32) + branch
    squares = jnp.sum(stream * stream, axis=-1, keepdims=True)
    squares = squares + partner(squares)
    gain = lax.dynamic_slice_in_dim(norm_gain, core * width, width)
    normed = stream * lax.rsqrt(squares / (2 * width) + norm_eps) * gain
    normed = normed.astype(jnp.bfloat16)
    late = (late_u2, late_d2, late_d3, late_d1)

    own, ends, mids, last = feed_forward(normed, up_own, up_odd, down_own, late, inner, outer)
    middle = (z > 0) & (z < outer - 1)
    come = jnp.where(
        middle,
        ends[0].astype(jnp.float32) + mids[0].astype(jnp.float32),
        last.astype(jnp.float32),
    )
    return (stream + own.astype(jnp.float32) + come).astype(jnp.bfloat16)


def solution(mesh):
    in_specs = (
        P("sp", "tp"),
        P("sp", "tp"),
        P("sp", "tp"),
        P("sp"),
        P(),
        P(),
        P("sp", "tp"),
        P("tp", None),
        P(),
        P("sp", "tp"),
        P("tp", "sp"),
    )
    out_specs = P("sp", "tp")
    sp, tp = mesh.shape["sp"], mesh.shape["tp"]
    inner = KV // tp
    body = gather_body
    if tp == 2 and inner == 4 and sp % inner == 0 and sp // inner == 4:
        split = functools.partial(split_body, inner, sp // inner)

        def body(*args):
            return split(*args)

    return jax.shard_map(body, mesh=mesh, in_specs=in_specs, out_specs=out_specs, check_vma=False)
```

profile of v0, /device:TPU:0, one launch (start us, length us, event | category | flops | bytes accessed | tf_op | source)
XLA Modules:
  0.0 820.9 jit_solution(14284742850310325787)
XLA Ops:
  6.6 1.3 and_reduce_fusion
  7.9 1.3 convert_select_fusion
  9.3 0.6 fusion.31
  9.8 1.7 scatter.4
  11.6 1.8 sine_multiply_fusion
  13.4 8.4 %prepare.1 = bf16[4,512,512]{2,1,0:T(8,128)(2,1)} custom-call(bf16[512,1024]{1,0:T(8,128)(2,1)} %q_ref.1, bf16[512,512]{1,0:T(8,128)(2,1)} %k_ref.1, bf16[512,512]{1,0:T(8,128)(2,1)} %v_ref.1, f32[512,128]{1,0:T(8,128)} %get-tuple-element.64.cos_ref, f32[512,128]{1,0:T(8,128)} %get-tuple-element.63.sin_ref, f32[1,128]{1,0:T(1,128)} %bitcast.82, ...), custom_call_target="tpu_custom_call" | custom-call | flops 10240000 | bytes 4194304 | tf_op jit(solution)/shard_map/prepare/pallas_call | solution.py:205
  21.8 0.2 broadcast_in_dim.73
  22.0 1.4 copy-done.8
  23.4 1.2 fusion.14
  24.6 3.0 collective-permute-start
  27.6 1.5 collective-permute-start.2
  29.1 4.4 constant_dynamic-slice_fusion.3
  33.5 7.4 collective-permute-done
  41.0 13.5 %collective-permute-done.1 = bf16[528,512]{1,0:T(8,128)(2,1)} collective-permute-done((bf16[528,512]{1,0:T(8,128)(2,1)}, bf16[528,512]{1,0:T(8,128)(2,1)}, u32[]{:S(2)}, u32[]{:S(2)}) %collective-permute-start.1) | collective-permute-done | bytes 540704 | tf_op jit(solution)/shard_map/ppermute | solution.py:686
  54.4 1.1 bitcast_dynamic-update-slice_fusion.1
  55.7 1.3 slice_bitcast_fusion
  57.0 1.3 collective-permute-start.4
  58.3 5.6 collective-permute-start.3
  63.9 17.2 %collective-permute-done.4 = bf16[2112,256]{1,0:T(8,128)(2,1)} collective-permute-done((bf16[2112,256]{1,0:T(8,128)(2,1)S(1)}, bf16[2112,256]{1,0:T(8,128)(2,1)}, u32[]{:S(2)}, u32[]{:S(2)}) %collective-permute-start.4) | collective-permute-done | bytes 1081376 | tf_op jit(solution)/shard_map/ppermute | solution.py:695
  81.1 1.3 collective-permute-start.5
  82.4 5.5 collective-permute-start.7
  87.9 17.2 %collective-permute-done.5 = bf16[2112,256]{1,0:T(8,128)(2,1)} collective-permute-done((bf16[2112,256]{1,0:T(8,128)(2,1)}, bf16[2112,256]{1,0:T(8,128)(2,1)}, u32[]{:S(2)}, u32[]{:S(2)}) %collective-permute-start.5) | collective-permute-done | bytes 1081376 | tf_op jit(solution)/shard_map/ppermute | solution.py:695
  105.1 1.3 collective-permute-start.6
  106.4 4.2 constant_dynamic-slice_fusion
  110.6 4.6 collective-permute-start.8
  115.3 1.4 broadcast_select_fusion.1
  116.6 11.0 %collective-permute-done.6 = bf16[2112,256]{1,0:T(8,128)(2,1)S(1)} collective-permute-done((bf16[2112,256]{1,0:T(8,128)(2,1)}, bf16[2112,256]{1,0:T(8,128)(2,1)S(1)}, u32[]{:S(2)}, u32[]{:S(2)}) %collective-permute-start.6) | collective-permute-done | bytes 1081376 | tf_op jit(solution)/shard_map/ppermute | solution.py:695
  127.6 0.1 broadcast_select_fusion.2
  127.8 5.2 collective-permute-done.8
  132.9 1.4 broadcast_select_fusion
  134.3 2.3 pad_maximum_fusion.2
  136.8 2.4 collective-permute-start.14
  139.2 3.0 collective-permute-start.15
  142.2 20.9 %collective-permute-done.14 = bf16[256,2048]{1,0:T(8,128)(2,1)S(1)} collective-permute-done((bf16[256,2048]{1,0:T(8,128)(2,1)}, bf16[256,2048]{1,0:T(8,128)(2,1)S(1)}, u32[]{:S(2)}, u32[]{:S(2)}) %collective-permute-start.14) | collective-permute-done | bytes 1048608 | tf_op jit(solution)/shard_map/ppermute | solution.py:686
  163.1 16.9 %collective-permute-done.15 = bf16[256,2048]{1,0:T(8,128)(2,1)S(1)} collective-permute-done((bf16[256,2048]{1,0:T(8,128)(2,1)S(1)}, bf16[256,2048]{1,0:T(8,128)(2,1)S(1)}, u32[]{:S(2)}, u32[]{:S(2)}) %collective-permute-start.15) | collective-permute-done | bytes 1048608 | tf_op jit(solution)/shard_map/ppermute | solution.py:686
  180.0 1.6 pad_maximum_fusion.3
  181.6 7.3 constant_dynamic-slice_fusion.12
  189.0 0.2 slice.67
  189.2 1.0 copy-done.5
  190.2 0.3 copy-done.7
  190.5 0.3 copy-done.13
  190.9 0.6 gather_fusion
  191.9 0.4 copy.13.qdoc_ref
  192.3 0.2 convert_reduce_fusion
  192.6 54.5 %attention.1 = bf16[2048,256]{1,0:T(8,128)(2,1)S(1)} custom-call(s32[5,8]{1,0:T(8,128)S(1)} %stack.46.span_ref, bf16[2048,512]{1,0:T(8,128)(2,1)S(1)} %bitcast.58, bf16[16,528,256]{2,1,0:T(8,128)(2,1)} %bitcast.69, s32[2048,1]{1,0:T(8,128)S(1)} %copy.13.qdoc_ref, s32[16,1,512]{2,1,0:T(1,128)S(1)} %reshape_reshape.3.kdoc_ref), custom_call_target="tpu_custom_call" | custom-call | flops 8589934592 | bytes 4325376 | tf_op jit(solution)/shard_map/attention/pallas_call | solution.py:294
  247.2 1.5 collective-permute-start.11
  248.7 8.7 %collective-permute-start.10 = (bf16[512,256]{1,0:T(8,128)(2,1)S(1)}, bf16[512,256]{1,0:T(8,128)(2,1)S(1)}, u32[]{:S(2)}, u32[]{:S(2)}) collective-permute-start(bf16[512,256]{1,0:T(8,128)(2,1)S(1)} %get-tuple-element.61), channel_id=1, source_target_pairs={{0,4},{2,6},{4,0},{6,2},{8,12},{10,14},{12,8},{14,10},{16,20},{18,... | collective-permute-start | bytes 786440 | tf_op jit(solution)/shard_map/ppermute | solution.py:686
  257.4 1.4 collective-permute-start.9
  258.8 4.0 pad_maximum_fusion
  262.8 9.2 %collective-permute-done.10 = bf16[512,256]{1,0:T(8,128)(2,1)S(1)} collective-permute-done((bf16[512,256]{1,0:T(8,128)(2,1)S(1)}, bf16[512,256]{1,0:T(8,128)(2,1)S(1)}, u32[]{:S(2)}, u32[]{:S(2)}) %collective-permute-start.10) | collective-permute-done | bytes 262176 | tf_op jit(solution)/shard_map/ppermute | solution.py:686
  272.0 8.7 %collective-permute-done.9 = bf16[512,256]{1,0:T(8,128)(2,1)S(1)} collective-permute-done((bf16[512,256]{1,0:T(8,128)(2,1)S(1)}, bf16[512,256]{1,0:T(8,128)(2,1)S(1)}, u32[]{:S(2)}, u32[]{:S(2)}) %collective-permute-start.9) | collective-permute-done | bytes 262176 | tf_op jit(solution)/shard_map/ppermute | solution.py:686
  280.7 8.2 %convolution_convert_fusion = bf16[512,4096]{1,0:T(8,128)(2,1)S(1)} fusion(bf16[1024,4096]{1,0:T(8,128)(2,1)} %pad_maximum_fusion, bf16[512,256]{1,0:T(8,128)(2,1)S(1)} %collective-permute-done.11, bf16[512,256]{1,0:T(8,128)(2,1)S(1)} %collective-permute-done.10, bf16[512,256]{1,0:T(8,128)(2,1)S(1)} %collective-permute-done.9, ...), kind=kOutput, calls=%fused_computation.2 | convolution fusion | flops 4301258752 | bytes 13631488 | tf_op jit(solution)/shard_map/dot_general | solution.py:769
  288.9 2.0 copy-done.1
  290.9 1.6 constant_dynamic-slice_fusion.8
  292.5 2.8 collective-permute-start.17
  295.4 1.5 collective-permute-start.19
  296.9 3.2 multiply_reduce_fusion
  300.2 0.2 collective-permute-start.13
  300.4 1.0 collective-permute-done.13
  301.4 5.0 multiply_convert_fusion.normed_ref
  306.5 58.0 %collective-permute-done.16.late_u2 = bf16[256,2048]{1,0:T(8,128)(2,1)} collective-permute-done((bf16[256,2048]{1,0:T(8,128)(2,1)S(1)}, bf16[256,2048]{1,0:T(8,128)(2,1)}, u32[]{:S(2)}, u32[]{:S(2)}) %collective-permute-start.16) | collective-permute-done | bytes 1048608 | tf_op jit(solution)/shard_map/ppermute | solution.py:686
  364.5 44.5 %collective-permute-done.17.late_d2 = bf16[2048,256]{1,0:T(8,128)(2,1)} collective-permute-done((bf16[2048,256]{1,0:T(8,128)(2,1)}, bf16[2048,256]{1,0:T(8,128)(2,1)}, u32[]{:S(2)}, u32[]{:S(2)}) %collective-permute-start.17) | collective-permute-done | bytes 1048608 | tf_op jit(solution)/shard_map/ppermute | solution.py:686
  409.0 397.6 %feed_forward.1 = (bf16[512,2048]{1,0:T(8,128)(2,1)}, bf16[3,512,2048]{2,1,0:T(8,128)(2,1)}, bf16[2,512,2048]{2,1,0:T(8,128)(2,1)}, bf16[512,2048]{1,0:T(8,128)(...) custom-call(bf16[512,2048]{1,0:T(8,128)(2,1)} %multiply_convert_fusi, ...), custom_call_target="tpu_custom_call" | custom-call | flops 68719476736 | tf_op jit(solution)/shard_map/feed_forward/pallas_call | solution.py:634
  806.6 7.7 fusion.1
  (75 shorter events, 1.2 us)
Async XLA Ops:
  6.5 402.4 %all-gather.7.cloned.1.call-start = ((), (), s32[]{:S(2)}) async-start(), calls=%async_computation | async-start | bytes 5242880 | tf_op jit(solution)/shard_map/all_gather | solution.py:712
  21.8 1.6 copy-start.8
  24.6 16.3 %collective-permute-start = (bf16[528,512]{1,0:T(8,128)(2,1)}, bf16[528,512]{1,0:T(8,128)(2,1)S(1)}, u32[]{:S(2)}, u32[]{:S(2)}) collective-permute-start(bf16[528,512]{1,0:T(8,128)(2,1)} %get-tuple-element.56), channel_id=1, source_target_pairs={{0,2},{2,0},{4,6},{6,4},{8,10},{10,8},{12,14},{14,12},{16,18},{18,... | collective-permute-start | bytes 1622024 | tf_op jit(solution)/shard_map/ppermute | solution.py:686
  27.6 27.9 %collective-permute-start.2 = (bf16[528,512]{1,0:T(8,128)(2,1)}, bf16[528,512]{1,0:T(8,128)(2,1)S(1)}, u32[]{:S(2)}, u32[]{:S(2)}) collective-permute-start(bf16[528,512]{1,0:T(8,128)(2,1)} %get-tuple-element.55), channel_id=1, source_target_pairs={{0,6},{2,4},{4,2},{6,0},{8,14},{10,12},{12,10},{14,8},{16,22},{18,... | collective-permute-start | bytes 1622024 | tf_op jit(solution)/shard_map/ppermute | solution.py:686
  29.1 25.4 %collective-permute-start.1 = (bf16[528,512]{1,0:T(8,128)(2,1)}, bf16[528,512]{1,0:T(8,128)(2,1)}, u32[]{:S(2)}, u32[]{:S(2)}) collective-permute-start(bf16[528,512]{1,0:T(8,128)(2,1)} %get-tuple-element.57), channel_id=1, source_target_pairs={{0,4},{2,6},{4,0},{6,2},{8,12},{10,14},{12,8},{14,10},{16,20},{18,... | collective-permute-start | bytes 1622024 | tf_op jit(solution)/shard_map/ppermute | solution.py:686
  55.6 55.0 %copy-start.2 = (bf16[4,528,512]{2,1,0:T(8,128)(2,1)}, bf16[4,528,512]{2,1,0:T(8,128)(2,1)S(1)}, u32[]{:S(2)}) copy-start(bf16[4,528,512]{2,1,0:T(8,128)(2,1)S(1)} %bitcast_dynamic-update-slice_fusion) | copy-start | bytes 6488068
  55.6 353.3 %all-gather.11.cloned.1.call-start = ((), (), s32[]{:S(2)}) async-start(), calls=%async_computation.2 | async-start | bytes 5242880 | tf_op jit(solution)/shard_map/all_gather | solution.py:712
  57.0 24.1 %collective-permute-start.4 = (bf16[2112,256]{1,0:T(8,128)(2,1)S(1)}, bf16[2112,256]{1,0:T(8,128)(2,1)}, u32[]{:S(2)}, u32[]{:S(2)}) collective-permute-start(bf16[2112,256]{1,0:T(8,128)(2,1)S(1)} %bitcast.66), channel_id=1, source_target_pairs={{8,0},{10,2},{12,4},{14,6},{16,8},{18,10},{20,12},{22,14},{24,16},... | collective-permute-start | bytes 3244040 | tf_op jit(solution)/shard_map/ppermute | solution.py:695
  58.3 24.1 %collective-permute-start.3 = (bf16[2112,256]{1,0:T(8,128)(2,1)S(1)}, bf16[2112,256]{1,0:T(8,128)(2,1)}, u32[]{:S(2)}, u32[]{:S(2)}) collective-permute-start(bf16[2112,256]{1,0:T(8,128)(2,1)S(1)} %bitcast.67), channel_id=1, source_target_pairs={{0,8},{2,10},{4,12},{6,14},{8,16},{10,18},{12,20},{14,22},{16,24},... | collective-permute-start | bytes 3244040 | tf_op jit(solution)/shard_map/ppermute | solution.py:695
  81.1 24.0 %collective-permute-start.5 = (bf16[2112,256]{1,0:T(8,128)(2,1)}, bf16[2112,256]{1,0:T(8,128)(2,1)}, u32[]{:S(2)}, u32[]{:S(2)}) collective-permute-start(bf16[2112,256]{1,0:T(8,128)(2,1)} %collective-permute-done.4), channel_id=1, source_target_pairs={{8,0},{10,2},{12,4},{14,6},{16,8},{18,10},{20,12},{22,14},{24,16},... | collective-permute-start | bytes 3244040 | tf_op jit(solution)/shard_map/ppermute | solution.py:695
  82.4 28.2 %collective-permute-start.7 = (bf16[2112,256]{1,0:T(8,128)(2,1)}, bf16[2112,256]{1,0:T(8,128)(2,1)}, u32[]{:S(2)}, u32[]{:S(2)}) collective-permute-start(bf16[2112,256]{1,0:T(8,128)(2,1)} %collective-permute-done.3), channel_id=1, source_target_pairs={{0,8},{2,10},{4,12},{6,14},{8,16},{10,18},{12,20},{14,22},{16,24},... | collective-permute-start | bytes 3244040 | tf_op jit(solution)/shard_map/ppermute | solution.py:695
  105.1 22.5 %collective-permute-start.6 = (bf16[2112,256]{1,0:T(8,128)(2,1)}, bf16[2112,256]{1,0:T(8,128)(2,1)S(1)}, u32[]{:S(2)}, u32[]{:S(2)}) collective-permute-start(bf16[2112,256]{1,0:T(8,128)(2,1)} %collective-permute-done.5), channel_id=1, source_target_pairs={{8,0},{10,2},{12,4},{14,6},{16,8},{18,10},{20,12},{22,14},{24,16},... | collective-permute-start | bytes 3244040 | tf_op jit(solution)/shard_map/ppermute | solution.py:695
  110.6 22.3 %collective-permute-start.8 = (bf16[2112,256]{1,0:T(8,128)(2,1)}, bf16[2112,256]{1,0:T(8,128)(2,1)S(1)}, u32[]{:S(2)}, u32[]{:S(2)}) collective-permute-start(bf16[2112,256]{1,0:T(8,128)(2,1)} %collective-permute-done.7), channel_id=1, source_target_pairs={{0,8},{2,10},{4,12},{6,14},{8,16},{10,18},{12,20},{14,22},{16,24},... | collective-permute-start | bytes 3244040 | tf_op jit(solution)/shard_map/ppermute | solution.py:695
  127.7 8.9 %copy-start.4 = (bf16[2112,256]{1,0:T(8,128)(2,1)}, bf16[2112,256]{1,0:T(8,128)(2,1)S(1)}, u32[]{:S(2)}) copy-start(bf16[2112,256]{1,0:T(8,128)(2,1)S(1)} %broadcast_select_fusion.2) | copy-start | bytes 3244036
  134.3 2.4 copy-start.6
  134.3 4.9 copy-start.15
  136.7 272.3 %all-gather.9.cloned.1.call-start = ((), (), s32[]{:S(2)}) async-start(), calls=%async_computation.1 | async-start | bytes 10485760 | tf_op jit(solution)/shard_map/all_gather | solution.py:712
  136.8 26.3 %collective-permute-start.14 = (bf16[256,2048]{1,0:T(8,128)(2,1)}, bf16[256,2048]{1,0:T(8,128)(2,1)S(1)}, u32[]{:S(2)}, u32[]{:S(2)}) collective-permute-start(bf16[256,2048]{1,0:T(8,128)(2,1)} %get-tuple-element.50), channel_id=1, source_target_pairs={{0,8},{2,10},{4,12},{6,14},{8,0},{10,2},{12,4},{14,6},{16,24},{18,... | collective-permute-start | bytes 3145736 | tf_op jit(solution)/shard_map/ppermute | solution.py:686
  139.2 40.8 %collective-permute-start.15 = (bf16[256,2048]{1,0:T(8,128)(2,1)S(1)}, bf16[256,2048]{1,0:T(8,128)(2,1)S(1)}, u32[]{:S(2)}, u32[]{:S(2)}) collective-permute-start(bf16[256,2048]{1,0:T(8,128)(2,1)S(1)} %copy-done.15), channel_id=1, source_target_pairs={{0,24},{2,26},{4,28},{6,30},{8,16},{10,18},{12,20},{14,22},{16,8},... | collective-permute-start | bytes 3145736 | tf_op jit(solution)/shard_map/ppermute | solution.py:686
  181.6 7.3 copy-start.3
  189.0 1.2 copy-start.5
  189.0 1.6 copy-start.7
  189.0 1.9 copy-start.13
  192.6 66.2 %copy-start.10 = (bf16[256,4096]{1,0:T(8,128)(2,1)S(1)}, bf16[256,4096]{1,0:T(8,128)(2,1)}, u32[]{:S(2)}) copy-start(bf16[256,4096]{1,0:T(8,128)(2,1)} %get-tuple-element.42) | copy-start | bytes 6291460
  192.6 66.2 %copy-start.11 = (bf16[256,4096]{1,0:T(8,128)(2,1)S(1)}, bf16[256,4096]{1,0:T(8,128)(2,1)}, u32[]{:S(2)}) copy-start(bf16[256,4096]{1,0:T(8,128)(2,1)} %get-tuple-element.43) | copy-start | bytes 6291460
  192.6 66.2 %copy-start.12 = (bf16[256,4096]{1,0:T(8,128)(2,1)S(1)}, bf16[256,4096]{1,0:T(8,128)(2,1)}, u32[]{:S(2)}) copy-start(bf16[256,4096]{1,0:T(8,128)(2,1)} %get-tuple-element.44) | copy-start | bytes 6291460
  247.1 11.7 %copy-start.9 = (bf16[256,4096]{1,0:T(8,128)(2,1)S(1)}, bf16[256,4096]{1,0:T(8,128)(2,1)}, u32[]{:S(2)}) copy-start(bf16[256,4096]{1,0:T(8,128)(2,1)} %get-tuple-element.41) | copy-start | bytes 6291460
  247.2 15.6 %collective-permute-start.11 = (bf16[512,256]{1,0:T(8,128)(2,1)S(1)}, bf16[512,256]{1,0:T(8,128)(2,1)S(1)}, u32[]{:S(2)}, u32[]{:S(2)}) collective-permute-start(bf16[512,256]{1,0:T(8,128)(2,1)S(1)} %get-tuple-element.60), channel_id=1, source_target_pairs={{0,6},{2,4},{4,2},{6,0},{8,14},{10,12},{12,10},{14,8},{16,22},{18,... | collective-permute-start | bytes 786440 | tf_op jit(solution)/shard_map/ppermute | solution.py:686
  248.7 23.3 %collective-permute-start.10 = (bf16[512,256]{1,0:T(8,128)(2,1)S(1)}, bf16[512,256]{1,0:T(8,128)(2,1)S(1)}, u32[]{:S(2)}, u32[]{:S(2)}) collective-permute-start(bf16[512,256]{1,0:T(8,128)(2,1)S(1)} %get-tuple-element.61), channel_id=1, source_target_pairs={{0,4},{2,6},{4,0},{6,2},{8,12},{10,14},{12,8},{14,10},{16,20},{18,... | collective-permute-start | bytes 786440 | tf_op jit(solution)/shard_map/ppermute | solution.py:686
  257.4 23.3 %collective-permute-start.9 = (bf16[512,256]{1,0:T(8,128)(2,1)S(1)}, bf16[512,256]{1,0:T(8,128)(2,1)S(1)}, u32[]{:S(2)}, u32[]{:S(2)}) collective-permute-start(bf16[512,256]{1,0:T(8,128)(2,1)S(1)} %get-tuple-element.62), channel_id=1, source_target_pairs={{0,2},{2,0},{4,6},{6,4},{8,10},{10,8},{12,14},{14,12},{16,18},{18,... | collective-permute-start | bytes 786440 | tf_op jit(solution)/shard_map/ppermute | solution.py:686
  288.9 2.0 copy-start.1
  290.9 1.6 copy-start.14
  290.9 6.1 copy-start
  292.4 4.5 collective-permute-start.12
  292.4 72.0 %collective-permute-start.16 = (bf16[256,2048]{1,0:T(8,128)(2,1)S(1)}, bf16[256,2048]{1,0:T(8,128)(2,1)}, u32[]{:S(2)}, u32[]{:S(2)}) collective-permute-start(bf16[256,2048]{1,0:T(8,128)(2,1)S(1)} %copy-done.14), channel_id=1, source_target_pairs={{0,16},{2,18},{4,20},{6,22},{8,24},{10,26},{12,28},{14,30},{16,0},... | collective-permute-start | bytes 3145736 | tf_op jit(solution)/shard_map/ppermute | solution.py:686
  292.4 9.0 %dynamic-slice-start = ((f32[4096]{0:T(1024)}, s32[]{:T(128)}), f32[2048]{0:T(1024)S(1)}, s32[]{:S(2)}) async-start(f32[4096]{0:T(1024)} %param.21, s32[]{:T(128)} %select_n.195), calls=%async_computation.3 | async-start | bytes 16896 | tf_op jit(solution)/shard_map/dynamic_slice | solution.py:777
  292.5 72.0 %collective-permute-start.18 = (bf16[2048,256]{1,0:T(8,128)(2,1)}, bf16[2048,256]{1,0:T(8,128)(2,1)}, u32[]{:S(2)}, u32[]{:S(2)}) collective-permute-start(bf16[2048,256]{1,0:T(8,128)(2,1)} %get-tuple-element.35), channel_id=1, source_target_pairs={{0,24},{2,26},{4,28},{6,30},{8,16},{10,18},{12,20},{14,22},{16,8},... | collective-permute-start | bytes 3145736 | tf_op jit(solution)/shard_map/ppermute | solution.py:686
  292.5 116.4 %collective-permute-start.17 = (bf16[2048,256]{1,0:T(8,128)(2,1)}, bf16[2048,256]{1,0:T(8,128)(2,1)}, u32[]{:S(2)}, u32[]{:S(2)}) collective-permute-start(bf16[2048,256]{1,0:T(8,128)(2,1)} %get-tuple-element.34), channel_id=1, source_target_pairs={{0,16},{2,18},{4,20},{6,22},{8,24},{10,26},{12,28},{14,30},{16,0},... | collective-permute-start | bytes 3145736 | tf_op jit(solution)/shard_map/ppermute | solution.py:686
  295.4 113.6 %collective-permute-start.19 = (bf16[2048,256]{1,0:T(8,128)(2,1)}, bf16[2048,256]{1,0:T(8,128)(2,1)}, u32[]{:S(2)}, u32[]{:S(2)}) collective-permute-start(bf16[2048,256]{1,0:T(8,128)(2,1)} %get-tuple-element.36), channel_id=1, source_target_pairs={{0,8},{2,10},{4,12},{6,14},{8,0},{10,2},{12,4},{14,6},{16,24},{18,... | collective-permute-start | bytes 3145736 | tf_op jit(solution)/shard_map/ppermute | solution.py:686
  300.2 1.2 collective-permute-start.13
Sparse Core Ops, SparseCore 0:
  55.8 52.8 all-gather.6
  136.8 57.1 all-gather.10
  195.9 107.2 all-gather.8
where the time goes:
time: 822 us; the launch traced here: 821 us
  Pallas kernels  461 us (56%)
  waiting for transfers between devices  231 us (28%)
  starting transfers between devices  45.7 us (6%)
  other arithmetic  32.7 us (4%)
  local copies, waits for them, and re-layouts  29.3 us (4%)
  between operations  13.5 us (2%)
  matrix products  8.22 us (1%)
    pallas_call x1, Pallas kernels, feed_forward(): pl.pallas_call(functools.partial(feed_kernel, outer, inner, tok, width, u...  398 us
    ppermute x12, waiting for transfers between devices, flip(): return lax.ppermute(array, 'sp', [(s, s ^ bits) for s in range(size)])  179 us
    pallas_call x1, Pallas kernels, attention(): pl.pallas_call(functools.partial(attend_kernel, group, key_block, slots),...  54.5 us
    ppermute x6, waiting for transfers between devices, line(): return lax.ppermute(array, 'sp', pairs)  50.6 us
    ppermute x12, starting transfers between devices, flip(): return lax.ppermute(array, 'sp', [(s, s ^ bits) for s in range(size)])  25.9 us
    ppermute x6, starting transfers between devices, line(): return lax.ppermute(array, 'sp', pairs)  19.5 us
  transfers between devices with their start and end apart: 23, of which 13 were waited for; matrix products, arithmetic and copies ran while one was open for 6% of the time, Pallas kernels for 7%

commit v1 on v0

--- a/solution.py
+++ b/solution.py
@@ -310,7 +310,7 @@
     outer, inner, tok, width, units,
     normed_ref, up_own, up_odd, down_own, late_u2, late_d2, late_d3, late_d1,
     own_ref, ends_ref, mids_ref, last_ref, tok_a, tok_b, given_s, given_r, send_e, send_x, send_l, land_u, land_d,
-    up_v, down_v, tok_v, sq_v, stage_v, recv_v, add_v, sum_v,
+    up_v, down_v, tok_v, sq_v, stage_v, recv_v, recv_w, add_v, sum_v,
     way_s, way_r, pair_s, pair_r, give_s, give_r, e_s, e_r, x_s, x_r, l_s, l_r, w_s, w_r, loc, big,
 ):
     me = lax.axis_index("sp")
@@ -320,7 +320,8 @@
     mid = ((z + 1) // 2) % 2
     near = (z + 1 - 2 * (z % 2)) * inner + i
     across = (outer - 1 - z) * inner + i
-    half = tok // 2
+    parts = 4
+    half = tok // parts
 
     barrier = pltpu.get_barrier_semaphore()
     beside = [{"sp": z * inner + i + bit - 2 * bit * ((i // bit) % 2)} for bit in (1, 2)]
@@ -471,32 +472,36 @@
 
     chunk = 128
 
-    def total(q, start, extra):
+    def total(q, share, start, extra):
         rows = pl.ds(start, chunk)
         value = up_v[keep_rows(q, start, chunk)].astype(jnp.float32)
-        value = value + recv_v[rows].astype(jnp.float32)
+        value = value + share[rows].astype(jnp.float32)
         if extra:
             value = value + add_v[rows].astype(jnp.float32)
         return value
 
+    def load_share(q, share):
+        given_pair(q).wait_recv()
+        local(given_r.at[q], share, loc.at[3])
+
+    def piece_on(h, q, share, extra, wait, out, copies):
+        rows = pl.ds(h * half, half)
+        if extra is not None:
+            wait(h)
+            local(extra.at[rows], add_v.at[rows], loc.at[4])
+
+        @pl.loop(0, half // chunk)
+        def _(n):
+            start = pl.multiple_of(h * half + n * chunk, chunk)
+            sum_v[pl.ds(start, chunk)] = total(q, share, start, extra is not None).astype(jnp.bfloat16)
+
+        local(sum_v.at[rows], out.at[rows], loc.at[5])
+        copies(h).start()
+
     def pass_on(q, extra, wait, out, copies):
-        given_pair(q).wait_recv()
-        one = pltpu.make_async_copy(given_r.at[q], recv_v, loc.at[3])
-        one.start()
-        one.wait()
-        for h in range(2):
-            rows = pl.ds(h * half, half)
-            if extra is not None:
-                wait(h)
-                local(extra.at[rows], add_v.at[rows], loc.at[4])
-
-            @pl.loop(0, half // chunk)
-            def _(n):
-                start = pl.multiple_of(h * half + n * chunk, chunk)
-                sum_v[pl.ds(start, chunk)] = total(q, start, extra is not None).astype(jnp.bfloat16)
-
-            local(sum_v.at[rows], out.at[rows], loc.at[5])
-            copies(h).start()
+        load_share(q, recv_v)
+        for h in range(parts):
+            piece_on(h, q, recv_v, extra, wait, out, copies)
 
     def halves(src, dst, send, recv, peer):
         def copy(h):
@@ -529,20 +534,16 @@
         copy.wait()
     hide(0, True)
     hide(1)
+    arrived(2)
+
+    @pl.when(mid == 1)
+    def _():
+        far_near.start()
+
     forward_item(2)
+    landed = land_item(1)
     forward_item(3)
-    landed = land_item(1)
-
-    @pl.when(mid == 0)
-    def _():
-        arrived(2)
-
     hide(2 + mid)
-
-    @pl.when(mid == 1)
-    def _():
-        arrived(2)
-        far_near.start()
 
     @pl.when(mid == 0)
     def _():
@@ -575,8 +576,15 @@
     @pl.when(mid == 1)
     def _():
         pass_on(3, ends_ref.at[1], lambda h: to_mid[1](h).wait_recv(), send_x.at[0], to_other[0])
-        pass_on(2, ends_ref.at[2], lambda h: to_mid[2](h).wait_recv(), send_x.at[1], to_other[1])
-        pass_on(1, mids_ref.at[1], lambda h: to_other[1](h).wait_recv(), send_l, to_end)
+        load_share(2, recv_v)
+        load_share(1, recv_w)
+        onward = (2, recv_v, ends_ref.at[2], lambda h: to_mid[2](h).wait_recv(), send_x.at[1], to_other[1])
+        home = (1, recv_w, mids_ref.at[1], lambda h: to_other[1](h).wait_recv(), send_l, to_end)
+        for h in range(parts):
+            piece_on(h, *onward)
+            if h:
+                piece_on(h - 1, *home)
+        piece_on(parts - 1, *home)
 
     given_pair(0).wait_recv()
     local(given_r.at[0], recv_v, loc.at[3])
@@ -584,13 +592,13 @@
     @pl.loop(0, tok // chunk)
     def _(n):
         start = pl.multiple_of(n * chunk, chunk)
-        sum_v[pl.ds(start, chunk)] = total(0, start, False).astype(jnp.bfloat16)
+        sum_v[pl.ds(start, chunk)] = total(0, recv_v, start, False).astype(jnp.bfloat16)
 
     local(sum_v, own_ref, loc.at[5])
 
     @pl.when(mid == 0)
     def _():
-        for h in range(2):
+        for h in range(parts):
             to_end(h).wait_recv()
             for n in range(3):
                 to_mid[n](h).wait_send()
@@ -601,7 +609,7 @@
         near_across.wait_send()
         across_near.wait_send()
         far_near.wait_send()
-        for h in range(2):
+        for h in range(parts):
             to_mid[0](h).wait_recv()
             to_other[0](h).wait_recv()
             for n in range(2):
@@ -645,8 +653,9 @@
             vmem(tok, width),
             vmem(tok, width),
             vmem(tok, width),
+            vmem(tok, width),
             dma((5,)), dma((outer,)), dma((outer,)), dma((outer,)), dma((outer,)), dma((outer,)),
-            dma((3, 2)), dma((3, 2)), dma((2, 2)), dma((2, 2)), dma((2,)), dma((2,)),
+            dma((3, 4)), dma((3, 4)), dma((2, 4)), dma((2, 4)), dma((4,)), dma((4,)),
             dma((4, inner - 1)), dma((4, inner - 1)), dma((6,)), dma((2, outer, inner)),
         ],
         compiler_params=pltpu.CompilerParams(

time: 822 us -> 767 us (0.933)
  Pallas kernels: 461 us -> 405 us
    pallas_call x1, Pallas kernels: 398 us -> 342 us  [feed_forward(): pl.pallas_call(functools.partial(feed_kernel, outer, inner, tok, width, u...]
where the time goes in v1:
time: 767 us; the launch traced here: 765 us
  Pallas kernels  405 us (53%)
  waiting for transfers between devices  231 us (30%)
  starting transfers between devices  45.7 us (6%)
  other arithmetic  32.7 us (4%)
  local copies, waits for them, and re-layouts  29.3 us (4%)
  between operations  13.5 us (2%)
  matrix products  8.22 us (1%)
    pallas_call x1, Pallas kernels, feed_forward(): pl.pallas_call(functools.partial(feed_kernel, outer, inner, tok, width, u...  342 us
    ppermute x12, waiting for transfers between devices, flip(): return lax.ppermute(array, 'sp', [(s, s ^ bits) for s in range(size)])  179 us
    pallas_call x1, Pallas kernels, attention(): pl.pallas_call(functools.partial(attend_kernel, group, key_block, slots),...  54.5 us
    ppermute x6, waiting for transfers between devices, line(): return lax.ppermute(array, 'sp', pairs)  50.6 us
    ppermute x12, starting transfers between devices, flip(): return lax.ppermute(array, 'sp', [(s, s ^ bits) for s in range(size)])  25.9 us
    ppermute x6, starting transfers between devices, line(): return lax.ppermute(array, 'sp', pairs)  19.5 us
  transfers between devices with their start and end apart: 23, of which 13 were waited for; matrix products, arithmetic and copies ran while one was open for 6% of the time, Pallas kernels for 7%

profile of v1, /device:TPU:0, one launch (start us, length us, event | category | flops | bytes accessed | tf_op | source)
XLA Modules:
  0.0 765.4 jit_solution(11080436753598497401)
XLA Ops:
  6.6 1.3 and_reduce_fusion
  7.9 1.3 convert_select_fusion
  9.3 0.6 fusion.31
  9.8 1.7 scatter.4
  11.6 1.8 sine_multiply_fusion
  13.4 8.4 %prepare.1 = bf16[4,512,512]{2,1,0:T(8,128)(2,1)} custom-call(bf16[512,1024]{1,0:T(8,128)(2,1)} %q_ref.1, bf16[512,512]{1,0:T(8,128)(2,1)} %k_ref.1, bf16[512,512]{1,0:T(8,128)(2,1)} %v_ref.1, f32[512,128]{1,0:T(8,128)} %get-tuple-element.64.cos_ref, f32[512,128]{1,0:T(8,128)} %get-tuple-element.63.sin_ref, f32[1,128]{1,0:T(1,128)} %bitcast.82, ...), custom_call_target="tpu_custom_call" | custom-call | flops 10240000 | bytes 4194304 | tf_op jit(solution)/shard_map/prepare/pallas_call | solution.py:205
  21.8 0.2 broadcast_in_dim.73
  22.0 1.4 copy-done.8
  23.4 1.2 fusion.14
  24.6 3.0 collective-permute-start
  27.6 1.5 collective-permute-start.2
  29.1 4.4 constant_dynamic-slice_fusion.3
  33.5 7.4 collective-permute-done
  41.0 13.5 %collective-permute-done.1 = bf16[528,512]{1,0:T(8,128)(2,1)} collective-permute-done((bf16[528,512]{1,0:T(8,128)(2,1)}, bf16[528,512]{1,0:T(8,128)(2,1)}, u32[]{:S(2)}, u32[]{:S(2)}) %collective-permute-start.1) | collective-permute-done | bytes 540704 | tf_op jit(solution)/shard_map/ppermute | solution.py:695
  54.4 1.1 bitcast_dynamic-update-slice_fusion.1
  55.7 1.3 slice_bitcast_fusion
  57.0 1.3 collective-permute-start.4
  58.3 5.6 collective-permute-start.3
  63.9 17.2 %collective-permute-done.4 = bf16[2112,256]{1,0:T(8,128)(2,1)} collective-permute-done((bf16[2112,256]{1,0:T(8,128)(2,1)S(1)}, bf16[2112,256]{1,0:T(8,128)(2,1)}, u32[]{:S(2)}, u32[]{:S(2)}) %collective-permute-start.4) | collective-permute-done | bytes 1081376 | tf_op jit(solution)/shard_map/ppermute | solution.py:704
  81.1 1.3 collective-permute-start.5
  82.4 5.5 collective-permute-start.7
  87.9 17.2 %collective-permute-done.5 = bf16[2112,256]{1,0:T(8,128)(2,1)} collective-permute-done((bf16[2112,256]{1,0:T(8,128)(2,1)}, bf16[2112,256]{1,0:T(8,128)(2,1)}, u32[]{:S(2)}, u32[]{:S(2)}) %collective-permute-start.5) | collective-permute-done | bytes 1081376 | tf_op jit(solution)/shard_map/ppermute | solution.py:704
  105.1 1.3 collective-permute-start.6
  106.4 4.2 constant_dynamic-slice_fusion
  110.6 4.6 collective-permute-start.8
  115.3 1.4 broadcast_select_fusion.1
  116.6 11.0 %collective-permute-done.6 = bf16[2112,256]{1,0:T(8,128)(2,1)S(1)} collective-permute-done((bf16[2112,256]{1,0:T(8,128)(2,1)}, bf16[2112,256]{1,0:T(8,128)(2,1)S(1)}, u32[]{:S(2)}, u32[]{:S(2)}) %collective-permute-start.6) | collective-permute-done | bytes 1081376 | tf_op jit(solution)/shard_map/ppermute | solution.py:704
  127.6 0.1 broadcast_select_fusion.2
  127.8 5.2 collective-permute-done.8
  132.9 1.4 broadcast_select_fusion
  134.3 2.3 pad_maximum_fusion.2
  136.8 2.4 collective-permute-start.14
  139.2 3.0 collective-permute-start.15
  142.2 20.9 %collective-permute-done.14 = bf16[256,2048]{1,0:T(8,128)(2,1)S(1)} collective-permute-done((bf16[256,2048]{1,0:T(8,128)(2,1)}, bf16[256,2048]{1,0:T(8,128)(2,1)S(1)}, u32[]{:S(2)}, u32[]{:S(2)}) %collective-permute-start.14) | collective-permute-done | bytes 1048608 | tf_op jit(solution)/shard_map/ppermute | solution.py:695
  163.1 16.9 %collective-permute-done.15 = bf16[256,2048]{1,0:T(8,128)(2,1)S(1)} collective-permute-done((bf16[256,2048]{1,0:T(8,128)(2,1)S(1)}, bf16[256,2048]{1,0:T(8,128)(2,1)S(1)}, u32[]{:S(2)}, u32[]{:S(2)}) %collective-permute-start.15) | collective-permute-done | bytes 1048608 | tf_op jit(solution)/shard_map/ppermute | solution.py:695
  180.0 1.6 pad_maximum_fusion.3
  181.6 7.3 constant_dynamic-slice_fusion.12
  189.0 0.2 slice.67
  189.2 1.0 copy-done.5
  190.2 0.3 copy-done.7
  190.5 0.3 copy-done.13
  190.9 0.6 gather_fusion
  191.9 0.4 copy.13.qdoc_ref
  192.3 0.2 convert_reduce_fusion
  192.6 54.5 %attention.1 = bf16[2048,256]{1,0:T(8,128)(2,1)S(1)} custom-call(s32[5,8]{1,0:T(8,128)S(1)} %stack.46.span_ref, bf16[2048,512]{1,0:T(8,128)(2,1)S(1)} %bitcast.58, bf16[16,528,256]{2,1,0:T(8,128)(2,1)} %bitcast.69, s32[2048,1]{1,0:T(8,128)S(1)} %copy.13.qdoc_ref, s32[16,1,512]{2,1,0:T(1,128)S(1)} %reshape_reshape.3.kdoc_ref), custom_call_target="tpu_custom_call" | custom-call | flops 8589934592 | bytes 4325376 | tf_op jit(solution)/shard_map/attention/pallas_call | solution.py:294
  247.2 1.5 collective-permute-start.11
  248.7 8.7 %collective-permute-start.10 = (bf16[512,256]{1,0:T(8,128)(2,1)S(1)}, bf16[512,256]{1,0:T(8,128)(2,1)S(1)}, u32[]{:S(2)}, u32[]{:S(2)}) collective-permute-start(bf16[512,256]{1,0:T(8,128)(2,1)S(1)} %get-tuple-element.61), channel_id=1, source_target_pairs={{0,4},{2,6},{4,0},{6,2},{8,12},{10,14},{12,8},{14,10},{16,20},{18,... | collective-permute-start | bytes 786440 | tf_op jit(solution)/shard_map/ppermute | solution.py:695
  257.4 1.4 collective-permute-start.9
  258.8 4.0 pad_maximum_fusion
  262.8 9.2 %collective-permute-done.10 = bf16[512,256]{1,0:T(8,128)(2,1)S(1)} collective-permute-done((bf16[512,256]{1,0:T(8,128)(2,1)S(1)}, bf16[512,256]{1,0:T(8,128)(2,1)S(1)}, u32[]{:S(2)}, u32[]{:S(2)}) %collective-permute-start.10) | collective-permute-done | bytes 262176 | tf_op jit(solution)/shard_map/ppermute | solution.py:695
  272.0 8.7 %collective-permute-done.9 = bf16[512,256]{1,0:T(8,128)(2,1)S(1)} collective-permute-done((bf16[512,256]{1,0:T(8,128)(2,1)S(1)}, bf16[512,256]{1,0:T(8,128)(2,1)S(1)}, u32[]{:S(2)}, u32[]{:S(2)}) %collective-permute-start.9) | collective-permute-done | bytes 262176 | tf_op jit(solution)/shard_map/ppermute | solution.py:695
  280.7 8.2 %convolution_convert_fusion = bf16[512,4096]{1,0:T(8,128)(2,1)S(1)} fusion(bf16[1024,4096]{1,0:T(8,128)(2,1)} %pad_maximum_fusion, bf16[512,256]{1,0:T(8,128)(2,1)S(1)} %collective-permute-done.11, bf16[512,256]{1,0:T(8,128)(2,1)S(1)} %collective-permute-done.10, bf16[512,256]{1,0:T(8,128)(2,1)S(1)} %collective-permute-done.9, ...), kind=kOutput, calls=%fused_computation.2 | convolution fusion | flops 4301258752 | bytes 13631488 | tf_op jit(solution)/shard_map/dot_general | solution.py:778
  288.9 2.0 copy-done.1
  290.9 1.6 constant_dynamic-slice_fusion.8
  292.5 2.8 collective-permute-start.17
  295.4 1.5 collective-permute-start.19
  296.9 3.2 multiply_reduce_fusion
  300.2 0.2 collective-permute-start.13
  300.4 1.0 collective-permute-done.13
  301.4 5.0 multiply_convert_fusion.normed_ref
  306.5 58.0 %collective-permute-done.16.late_u2 = bf16[256,2048]{1,0:T(8,128)(2,1)} collective-permute-done((bf16[256,2048]{1,0:T(8,128)(2,1)S(1)}, bf16[256,2048]{1,0:T(8,128)(2,1)}, u32[]{:S(2)}, u32[]{:S(2)}) %collective-permute-start.16) | collective-permute-done | bytes 1048608 | tf_op jit(solution)/shard_map/ppermute | solution.py:695
  364.5 44.5 %collective-permute-done.17.late_d2 = bf16[2048,256]{1,0:T(8,128)(2,1)} collective-permute-done((bf16[2048,256]{1,0:T(8,128)(2,1)}, bf16[2048,256]{1,0:T(8,128)(2,1)}, u32[]{:S(2)}, u32[]{:S(2)}) %collective-permute-start.17) | collective-permute-done | bytes 1048608 | tf_op jit(solution)/shard_map/ppermute | solution.py:695
  409.0 342.2 %feed_forward.1 = (bf16[512,2048]{1,0:T(8,128)(2,1)}, bf16[3,512,2048]{2,1,0:T(8,128)(2,1)}, bf16[2,512,2048]{2,1,0:T(8,128)(2,1)}, bf16[512,2048]{1,0:T(8,128)(...) custom-call(bf16[512,2048]{1,0:T(8,128)(2,1)} %multiply_convert_fusi, ...), custom_call_target="tpu_custom_call" | custom-call | flops 68719476736 | tf_op jit(solution)/shard_map/feed_forward/pallas_call | solution.py:642
  751.2 7.7 %fusion.1 = bf16[512,2048]{1,0:T(8,128)(2,1)} fusion(bf16[512,2048]{1,0:T(8,128)(2,1)} %get-tuple-element.40, bf16[512,2048]{1,0:T(8,128)(2,1)} %get-tuple-element.37, bf16[2,512,2048]{2,1,0:T(8,128)(2,1)} %get-tuple-element.39, bf16[3,512,2048]{2,1,0:T(8,128)(2,1)} %get-tuple-element.38, pred[]{:T(512)S(6)} %and.95, ...), kind=kLoop, calls=%fused_computation.11 | loop fusion | flops 14680064 | bytes 16777220 | tf_op jit(solution)/shard_map/convert_element_type | solution.py:798
  (75 shorter events, 1.2 us)
Async XLA Ops:
  6.5 402.4 %all-gather.7.cloned.1.call-start = ((), (), s32[]{:S(2)}) async-start(), calls=%async_computation | async-start | bytes 5242880 | tf_op jit(solution)/shard_map/all_gather | solution.py:721
  21.8 1.6 copy-start.8
  24.6 16.3 %collective-permute-start = (bf16[528,512]{1,0:T(8,128)(2,1)}, bf16[528,512]{1,0:T(8,128)(2,1)S(1)}, u32[]{:S(2)}, u32[]{:S(2)}) collective-permute-start(bf16[528,512]{1,0:T(8,128)(2,1)} %get-tuple-element.56), channel_id=1, source_target_pairs={{0,2},{2,0},{4,6},{6,4},{8,10},{10,8},{12,14},{14,12},{16,18},{18,... | collective-permute-start | bytes 1622024 | tf_op jit(solution)/shard_map/ppermute | solution.py:695
  27.6 27.9 %collective-permute-start.2 = (bf16[528,512]{1,0:T(8,128)(2,1)}, bf16[528,512]{1,0:T(8,128)(2,1)S(1)}, u32[]{:S(2)}, u32[]{:S(2)}) collective-permute-start(bf16[528,512]{1,0:T(8,128)(2,1)} %get-tuple-element.55), channel_id=1, source_target_pairs={{0,6},{2,4},{4,2},{6,0},{8,14},{10,12},{12,10},{14,8},{16,22},{18,... | collective-permute-start | bytes 1622024 | tf_op jit(solution)/shard_map/ppermute | solution.py:695
  29.1 25.4 %collective-permute-start.1 = (bf16[528,512]{1,0:T(8,128)(2,1)}, bf16[528,512]{1,0:T(8,128)(2,1)}, u32[]{:S(2)}, u32[]{:S(2)}) collective-permute-start(bf16[528,512]{1,0:T(8,128)(2,1)} %get-tuple-element.57), channel_id=1, source_target_pairs={{0,4},{2,6},{4,0},{6,2},{8,12},{10,14},{12,8},{14,10},{16,20},{18,... | collective-permute-start | bytes 1622024 | tf_op jit(solution)/shard_map/ppermute | solution.py:695
  55.6 55.0 %copy-start.2 = (bf16[4,528,512]{2,1,0:T(8,128)(2,1)}, bf16[4,528,512]{2,1,0:T(8,128)(2,1)S(1)}, u32[]{:S(2)}) copy-start(bf16[4,528,512]{2,1,0:T(8,128)(2,1)S(1)} %bitcast_dynamic-update-slice_fusion) | copy-start | bytes 6488068
  55.6 353.3 %all-gather.11.cloned.1.call-start = ((), (), s32[]{:S(2)}) async-start(), calls=%async_computation.2 | async-start | bytes 5242880 | tf_op jit(solution)/shard_map/all_gather | solution.py:721
  57.0 24.1 %collective-permute-start.4 = (bf16[2112,256]{1,0:T(8,128)(2,1)S(1)}, bf16[2112,256]{1,0:T(8,128)(2,1)}, u32[]{:S(2)}, u32[]{:S(2)}) collective-permute-start(bf16[2112,256]{1,0:T(8,128)(2,1)S(1)} %bitcast.66), channel_id=1, source_target_pairs={{8,0},{10,2},{12,4},{14,6},{16,8},{18,10},{20,12},{22,14},{24,16},... | collective-permute-start | bytes 3244040 | tf_op jit(solution)/shard_map/ppermute | solution.py:704
  58.3 24.1 %collective-permute-start.3 = (bf16[2112,256]{1,0:T(8,128)(2,1)S(1)}, bf16[2112,256]{1,0:T(8,128)(2,1)}, u32[]{:S(2)}, u32[]{:S(2)}) collective-permute-start(bf16[2112,256]{1,0:T(8,128)(2,1)S(1)} %bitcast.67), channel_id=1, source_target_pairs={{0,8},{2,10},{4,12},{6,14},{8,16},{10,18},{12,20},{14,22},{16,24},... | collective-permute-start | bytes 3244040 | tf_op jit(solution)/shard_map/ppermute | solution.py:704
  81.1 24.0 %collective-permute-start.5 = (bf16[2112,256]{1,0:T(8,128)(2,1)}, bf16[2112,256]{1,0:T(8,128)(2,1)}, u32[]{:S(2)}, u32[]{:S(2)}) collective-permute-start(bf16[2112,256]{1,0:T(8,128)(2,1)} %collective-permute-done.4), channel_id=1, source_target_pairs={{8,0},{10,2},{12,4},{14,6},{16,8},{18,10},{20,12},{22,14},{24,16},... | collective-permute-start | bytes 3244040 | tf_op jit(solution)/shard_map/ppermute | solution.py:704
  82.4 28.2 %collective-permute-start.7 = (bf16[2112,256]{1,0:T(8,128)(2,1)}, bf16[2112,256]{1,0:T(8,128)(2,1)}, u32[]{:S(2)}, u32[]{:S(2)}) collective-permute-start(bf16[2112,256]{1,0:T(8,128)(2,1)} %collective-permute-done.3), channel_id=1, source_target_pairs={{0,8},{2,10},{4,12},{6,14},{8,16},{10,18},{12,20},{14,22},{16,24},... | collective-permute-start | bytes 3244040 | tf_op jit(solution)/shard_map/ppermute | solution.py:704
  105.1 22.5 %collective-permute-start.6 = (bf16[2112,256]{1,0:T(8,128)(2,1)}, bf16[2112,256]{1,0:T(8,128)(2,1)S(1)}, u32[]{:S(2)}, u32[]{:S(2)}) collective-permute-start(bf16[2112,256]{1,0:T(8,128)(2,1)} %collective-permute-done.5), channel_id=1, source_target_pairs={{8,0},{10,2},{12,4},{14,6},{16,8},{18,10},{20,12},{22,14},{24,16},... | collective-permute-start | bytes 3244040 | tf_op jit(solution)/shard_map/ppermute | solution.py:704
  110.6 22.3 %collective-permute-start.8 = (bf16[2112,256]{1,0:T(8,128)(2,1)}, bf16[2112,256]{1,0:T(8,128)(2,1)S(1)}, u32[]{:S(2)}, u32[]{:S(2)}) collective-permute-start(bf16[2112,256]{1,0:T(8,128)(2,1)} %collective-permute-done.7), channel_id=1, source_target_pairs={{0,8},{2,10},{4,12},{6,14},{8,16},{10,18},{12,20},{14,22},{16,24},... | collective-permute-start | bytes 3244040 | tf_op jit(solution)/shard_map/ppermute | solution.py:704
  127.7 8.9 %copy-start.4 = (bf16[2112,256]{1,0:T(8,128)(2,1)}, bf16[2112,256]{1,0:T(8,128)(2,1)S(1)}, u32[]{:S(2)}) copy-start(bf16[2112,256]{1,0:T(8,128)(2,1)S(1)} %broadcast_select_fusion.2) | copy-start | bytes 3244036
  134.3 2.4 copy-start.6
  134.3 4.9 copy-start.15
  136.7 272.3 %all-gather.9.cloned.1.call-start = ((), (), s32[]{:S(2)}) async-start(), calls=%async_computation.1 | async-start | bytes 10485760 | tf_op jit(solution)/shard_map/all_gather | solution.py:721
  136.8 26.3 %collective-permute-start.14 = (bf16[256,2048]{1,0:T(8,128)(2,1)}, bf16[256,2048]{1,0:T(8,128)(2,1)S(1)}, u32[]{:S(2)}, u32[]{:S(2)}) collective-permute-start(bf16[256,2048]{1,0:T(8,128)(2,1)} %get-tuple-element.50), channel_id=1, source_target_pairs={{0,8},{2,10},{4,12},{6,14},{8,0},{10,2},{12,4},{14,6},{16,24},{18,... | collective-permute-start | bytes 3145736 | tf_op jit(solution)/shard_map/ppermute | solution.py:695
  139.2 40.8 %collective-permute-start.15 = (bf16[256,2048]{1,0:T(8,128)(2,1)S(1)}, bf16[256,2048]{1,0:T(8,128)(2,1)S(1)}, u32[]{:S(2)}, u32[]{:S(2)}) collective-permute-start(bf16[256,2048]{1,0:T(8,128)(2,1)S(1)} %copy-done.15), channel_id=1, source_target_pairs={{0,24},{2,26},{4,28},{6,30},{8,16},{10,18},{12,20},{14,22},{16,8},... | collective-permute-start | bytes 3145736 | tf_op jit(solution)/shard_map/ppermute | solution.py:695
  181.6 7.3 copy-start.3
  189.0 1.2 copy-start.5
  189.0 1.6 copy-start.7
  189.0 1.9 copy-start.13
  192.6 66.2 %copy-start.10 = (bf16[256,4096]{1,0:T(8,128)(2,1)S(1)}, bf16[256,4096]{1,0:T(8,128)(2,1)}, u32[]{:S(2)}) copy-start(bf16[256,4096]{1,0:T(8,128)(2,1)} %get-tuple-element.42) | copy-start | bytes 6291460
  192.6 66.2 %copy-start.11 = (bf16[256,4096]{1,0:T(8,128)(2,1)S(1)}, bf16[256,4096]{1,0:T(8,128)(2,1)}, u32[]{:S(2)}) copy-start(bf16[256,4096]{1,0:T(8,128)(2,1)} %get-tuple-element.43) | copy-start | bytes 6291460
  192.6 66.2 %copy-start.12 = (bf16[256,4096]{1,0:T(8,128)(2,1)S(1)}, bf16[256,4096]{1,0:T(8,128)(2,1)}, u32[]{:S(2)}) copy-start(bf16[256,4096]{1,0:T(8,128)(2,1)} %get-tuple-element.44) | copy-start | bytes 6291460
  247.1 11.7 %copy-start.9 = (bf16[256,4096]{1,0:T(8,128)(2,1)S(1)}, bf16[256,4096]{1,0:T(8,128)(2,1)}, u32[]{:S(2)}) copy-start(bf16[256,4096]{1,0:T(8,128)(2,1)} %get-tuple-element.41) | copy-start | bytes 6291460
  247.2 15.6 %collective-permute-start.11 = (bf16[512,256]{1,0:T(8,128)(2,1)S(1)}, bf16[512,256]{1,0:T(8,128)(2,1)S(1)}, u32[]{:S(2)}, u32[]{:S(2)}) collective-permute-start(bf16[512,256]{1,0:T(8,128)(2,1)S(1)} %get-tuple-element.60), channel_id=1, source_target_pairs={{0,6},{2,4},{4,2},{6,0},{8,14},{10,12},{12,10},{14,8},{16,22},{18,... | collective-permute-start | bytes 786440 | tf_op jit(solution)/shard_map/ppermute | solution.py:695
  248.7 23.3 %collective-permute-start.10 = (bf16[512,256]{1,0:T(8,128)(2,1)S(1)}, bf16[512,256]{1,0:T(8,128)(2,1)S(1)}, u32[]{:S(2)}, u32[]{:S(2)}) collective-permute-start(bf16[512,256]{1,0:T(8,128)(2,1)S(1)} %get-tuple-element.61), channel_id=1, source_target_pairs={{0,4},{2,6},{4,0},{6,2},{8,12},{10,14},{12,8},{14,10},{16,20},{18,... | collective-permute-start | bytes 786440 | tf_op jit(solution)/shard_map/ppermute | solution.py:695
  257.4 23.3 %collective-permute-start.9 = (bf16[512,256]{1,0:T(8,128)(2,1)S(1)}, bf16[512,256]{1,0:T(8,128)(2,1)S(1)}, u32[]{:S(2)}, u32[]{:S(2)}) collective-permute-start(bf16[512,256]{1,0:T(8,128)(2,1)S(1)} %get-tuple-element.62), channel_id=1, source_target_pairs={{0,2},{2,0},{4,6},{6,4},{8,10},{10,8},{12,14},{14,12},{16,18},{18,... | collective-permute-start | bytes 786440 | tf_op jit(solution)/shard_map/ppermute | solution.py:695
  288.9 2.0 copy-start.1
  290.9 1.6 copy-start.14
  290.9 6.1 copy-start
  292.4 4.5 collective-permute-start.12
  292.4 72.0 %collective-permute-start.16 = (bf16[256,2048]{1,0:T(8,128)(2,1)S(1)}, bf16[256,2048]{1,0:T(8,128)(2,1)}, u32[]{:S(2)}, u32[]{:S(2)}) collective-permute-start(bf16[256,2048]{1,0:T(8,128)(2,1)S(1)} %copy-done.14), channel_id=1, source_target_pairs={{0,16},{2,18},{4,20},{6,22},{8,24},{10,26},{12,28},{14,30},{16,0},... | collective-permute-start | bytes 3145736 | tf_op jit(solution)/shard_map/ppermute | solution.py:695
  292.4 9.0 %dynamic-slice-start = ((f32[4096]{0:T(1024)}, s32[]{:T(128)}), f32[2048]{0:T(1024)S(1)}, s32[]{:S(2)}) async-start(f32[4096]{0:T(1024)} %param.21, s32[]{:T(128)} %select_n.195), calls=%async_computation.3 | async-start | bytes 16896 | tf_op jit(solution)/shard_map/dynamic_slice | solution.py:786
  292.5 72.0 %collective-permute-start.18 = (bf16[2048,256]{1,0:T(8,128)(2,1)}, bf16[2048,256]{1,0:T(8,128)(2,1)}, u32[]{:S(2)}, u32[]{:S(2)}) collective-permute-start(bf16[2048,256]{1,0:T(8,128)(2,1)} %get-tuple-element.35), channel_id=1, source_target_pairs={{0,24},{2,26},{4,28},{6,30},{8,16},{10,18},{12,20},{14,22},{16,8},... | collective-permute-start | bytes 3145736 | tf_op jit(solution)/shard_map/ppermute | solution.py:695
  292.5 116.4 %collective-permute-start.17 = (bf16[2048,256]{1,0:T(8,128)(2,1)}, bf16[2048,256]{1,0:T(8,128)(2,1)}, u32[]{:S(2)}, u32[]{:S(2)}) collective-permute-start(bf16[2048,256]{1,0:T(8,128)(2,1)} %get-tuple-element.34), channel_id=1, source_target_pairs={{0,16},{2,18},{4,20},{6,22},{8,24},{10,26},{12,28},{14,30},{16,0},... | collective-permute-start | bytes 3145736 | tf_op jit(solution)/shard_map/ppermute | solution.py:695
  295.4 113.6 %collective-permute-start.19 = (bf16[2048,256]{1,0:T(8,128)(2,1)}, bf16[2048,256]{1,0:T(8,128)(2,1)}, u32[]{:S(2)}, u32[]{:S(2)}) collective-permute-start(bf16[2048,256]{1,0:T(8,128)(2,1)} %get-tuple-element.36), channel_id=1, source_target_pairs={{0,8},{2,10},{4,12},{6,14},{8,0},{10,2},{12,4},{14,6},{16,24},{18,... | collective-permute-start | bytes 3145736 | tf_op jit(solution)/shard_map/ppermute | solution.py:695
  300.2 1.2 collective-permute-start.13
Sparse Core Ops, SparseCore 0:
  55.8 52.8 all-gather.6
  136.8 57.1 all-gather.10
  195.9 107.2 all-gather.8
